TPU v7x, 32 devices: a whole 2x2x4 slice. The times are simulated.
32 devices in a mesh: fs: 8 (over z, y), tp: 4 (over x, core).
Axes of the slice: x: 2, y: 2, z: 4, core: 2. Of those that a mesh axis runs over, the one named last changes fastest.
Arguments:
- saved_inputs: bfloat16 [16384, 4096], P('fs'), may hold values from -6 to 6
- value_cot: bfloat16 [16384, 1024], P('fs', 'tp'), may hold values from -6 to 6
- gate_cot: bfloat16 [16384, 1024], P('fs', 'tp'), may hold values from -6 to 6
- point_inputs: bfloat16 [16384, 1024], P('fs'), may hold values from -6 to 6
- point_cot: bfloat16 [16384, 1024], P('fs', 'tp'), may hold values from -6 to 6
- master_value: float32 [4096, 1024], P('fs', 'tp'), may hold values from -6 to 6
- master_gate: float32 [4096, 1024], P('fs', 'tp'), may hold values from -6 to 6
- master_point: float32 [1024, 1024], P('fs', 'tp'), may hold values from -6 to 6
- factor_value: bfloat16 [4096, 256], P('fs'), may hold values from -160 to 160
- factor_gate: bfloat16 [4096, 256], P('fs'), may hold values from -160 to 160
- factor_point: bfloat16 [1024, 256], P('fs'), may hold values from -160 to 160
- first_value: float32 [256, 1024], P('fs', 'tp'), may hold values from -6 to 6
- first_gate: float32 [256, 1024], P('fs', 'tp'), may hold values from -6 to 6
- first_point: float32 [256, 1024], P('fs', 'tp'), may hold values from -6 to 6
- second_value: float32 [256, 1024], P('fs', 'tp'), may hold values from 0.2 to 2
- second_gate: float32 [256, 1024], P('fs', 'tp'), may hold values from 0.2 to 2
- second_point: float32 [256, 1024], P('fs', 'tp'), may hold values from 0.2 to 2
Outputs:
- new_value: float32 [4096, 1024], P('fs', 'tp')
- new_gate: float32 [4096, 1024], P('fs', 'tp')
- new_point: float32 [1024, 1024], P('fs', 'tp')
- copy_value: bfloat16 [4096, 1024], P(None, 'tp')
- copy_gate: bfloat16 [4096, 1024], P(None, 'tp')
- copy_point: bfloat16 [1024, 1024], P(None, 'tp')
- next_first_value: float32 [256, 1024], P('fs', 'tp')
- next_first_gate: float32 [256, 1024], P('fs', 'tp')
- next_first_point: float32 [256, 1024], P('fs', 'tp')
- next_second_value: float32 [256, 1024], P('fs', 'tp')
- next_second_gate: float32 [256, 1024], P('fs', 'tp')
- next_second_point: float32 [256, 1024], P('fs', 'tp')
All inputs are finite; a program needn't handle non-finite values.
Results may differ from a plain program's by a relative error of at most 0.0055.
Values may be sent and summed in bfloat16 or wider, within the bound.
A program may use at most 128 MiB of HBM per device.

v0:
```python
import jax
import jax.numpy as jnp
from jax import lax
from jax.sharding import PartitionSpec as P


def contract_rows(left, right):
    return lax.dot_general(
        left, right, (((0,), (0,)), ((), ())), preferred_element_type=jnp.float32
    )


def contract_split(projected, cot):
    upper = projected.astype(jnp.bfloat16)
    lower = (projected - upper.astype(jnp.float32)).astype(jnp.bfloat16)
    return contract_rows(upper, cot) + contract_rows(lower, cot)


def moments(low, first_old, second_old):
    first = 0.8 * first_old + 0.2 * low
    second = 0.9 * second_old + 0.1 * low * low
    return (first, second, first / (jnp.sqrt(second) + 1e-08))


def local(
    saved_inputs,
    value_cot,
    gate_cot,
    point_inputs,
    point_cot,
    master_value,
    master_gate,
    master_point,
    factor_value,
    factor_gate,
    factor_point,
    first_value,
    first_gate,
    first_point,
    second_value,
    second_gate,
    second_point,
):
    total = saved_inputs.shape[0] * lax.axis_size("fs")
    columns = saved_inputs
    proj_value = jnp.dot(
        columns,
        lax.all_gather(factor_value, "fs", axis=0, tiled=True),
        preferred_element_type=jnp.float32,
    )
    proj_gate = jnp.dot(
        columns,
        lax.all_gather(factor_gate, "fs", axis=0, tiled=True),
        preferred_element_type=jnp.float32,
    )
    columns = point_inputs
    proj_point = jnp.dot(
        columns,
        lax.all_gather(factor_point, "fs", axis=0, tiled=True),
        preferred_element_type=jnp.float32,
    )
    low_value = contract_split(proj_value, value_cot)
    low_gate = contract_split(proj_gate, gate_cot)
    low_point = contract_split(proj_point, point_cot)
    summed = (
        lax.psum_scatter(low_value, "fs", scatter_dimension=0, tiled=True),
        lax.psum_scatter(low_gate, "fs", scatter_dimension=0, tiled=True),
        lax.psum_scatter(low_point, "fs", scatter_dimension=0, tiled=True),
    )
    fv, sv, dv = moments(summed[0] / total, first_value, second_value)
    fg, sg, dg = moments(summed[1] / total, first_gate, second_gate)
    fpt, spt, dpt = moments(summed[2] / total, first_point, second_point)
    whole_v, whole_g, whole_p = (
        lax.all_gather(dv, "fs", axis=0, tiled=True),
        lax.all_gather(dg, "fs", axis=0, tiled=True),
        lax.all_gather(dpt, "fs", axis=0, tiled=True),
    )
    full_v = jnp.dot(factor_value.astype(jnp.float32), whole_v, precision=lax.Precision.HIGHEST)
    full_g = jnp.dot(factor_gate.astype(jnp.float32), whole_g, precision=lax.Precision.HIGHEST)
    full_p = jnp.dot(factor_point.astype(jnp.float32), whole_p, precision=lax.Precision.HIGHEST)
    squares = lax.psum(
        (jnp.sum(full_v * full_v), jnp.sum(full_g * full_g), jnp.sum(full_p * full_p)), ("fs", "tp")
    )
    spread = lax.axis_size("fs") * lax.axis_size("tp")
    entries_in = full_v.shape[0] * full_v.shape[1] * spread
    entries_point = full_p.shape[0] * full_p.shape[1] * spread
    new_v = master_value - 0.1 * lax.rsqrt(squares[0] / entries_in + 1e-06) * full_v
    new_g = master_gate - 0.1 * lax.rsqrt(squares[1] / entries_in + 1e-06) * full_g
    new_p = master_point - 0.1 * lax.rsqrt(squares[2] / entries_point + 1e-06) * full_p
    copy_v, copy_g, copy_p = (
        lax.all_gather(new_v.astype(jnp.bfloat16), "fs", axis=0, tiled=True),
        lax.all_gather(new_g.astype(jnp.bfloat16), "fs", axis=0, tiled=True),
        lax.all_gather(new_p.astype(jnp.bfloat16), "fs", axis=0, tiled=True),
    )
    return (new_v, new_g, new_p, copy_v, copy_g, copy_p, fv, fg, fpt, sv, sg, spt)


def solution(mesh):
    return jax.shard_map(
        local,
        mesh=mesh,
        in_specs=(
            P("fs", None),
            P("fs", "tp"),
            P("fs", "tp"),
            P("fs", None),
            P("fs", "tp"),
            P("fs", "tp"),
            P("fs", "tp"),
            P("fs", "tp"),
            P("fs", None),
            P("fs", None),
            P("fs", None),
            P("fs", "tp"),
            P("fs", "tp"),
            P("fs", "tp"),
            P("fs", "tp"),
            P("fs", "tp"),
            P("fs", "tp"),
        ),
        out_specs=(
            P("fs", "tp"),
            P("fs", "tp"),
            P("fs", "tp"),
            P(None, "tp"),
            P(None, "tp"),
            P(None, "tp"),
            P("fs", "tp"),
            P("fs", "tp"),
            P("fs", "tp"),
            P("fs", "tp"),
            P("fs", "tp"),
            P("fs", "tp"),
        ),
        check_vma=False,
    )
```

profile of v0, /device:TPU:0, one launch (start us, length us, event | category | flops | bytes accessed | tf_op | source)
XLA Modules:
  0.0 531.6 jit_solution(17776841322710641022)
XLA Ops:
  7.2 0.0 copy-start
  7.2 0.0 reduce-scatter.8.cloned.1.call-start
  7.2 33.4 %all_gather.31 = bf16[1024,256]{1,0:T(8,128)(2,1)S(1)} all-gather(bf16[128,256]{1,0:T(8,128)(2,1)} %param.27), channel_id=1, replica_groups=mesh['fs'=8,'tp'=4] {'fs'}, dimensions={0}, use_global_device_ids=true | all-gather | bytes 589824 | tf_op jit(solution)/shard_map/all_gather | solution.py:59
  40.6 3.5 fusion.14
  44.1 0.5 fusion.1
  44.6 0.0 copy-start.5
  44.6 0.0 copy-start.8
  44.6 0.0 copy-start.9
  44.6 1.2 convolution_add_fusion
  45.8 0.0 reduce-scatter.8.cloned.1.call-update
  45.8 0.0 all-gather.7.cloned.1.call-start
  45.9 0.7 all-gather.7.cloned.1.call-update
  46.6 0.0 all-gather.5.cloned.1.call-start
  46.6 0.7 all-gather.5.cloned.1.call-update
  47.3 0.0 reduce-scatter.6.cloned.1.call-start
  47.4 0.2 copy.29
  47.6 61.6 %reduce-scatter.8.cloned.1.call-done = f32[32,256]{1,0:T(8,128)} async-done(((f32[256,256]{1,0:T(8,128)}), f32[32,256]{1,0:T(8,128)}) %reduce-scatter.8.cloned.1.call-update) | async-done | bytes 32784 | tf_op jit(solution)/shard_map/reduce_scatter | solution.py:68
  109.2 1.4 add_divide_fusion
  110.6 31.4 %all_gather.32 = f32[256,256]{1,0:T(8,128)S(1)} all-gather(f32[32,256]{1,0:T(8,128)S(1)} %get-tuple-element.33), channel_id=1, replica_groups=mesh['fs'=8,'tp'=4] {'fs'}, dimensions={0}, use_global_device_ids=true | all-gather | bytes 294912 | tf_op jit(solution)/shard_map/all_gather | solution.py:76
  142.0 18.3 %all-gather.7.cloned.1.call-done = bf16[4096,256]{1,0:T(8,128)(2,1)} async-done(((bf16[512,256]{1,0:T(8,128)(2,1)}), bf16[4096,256]{1,0:T(8,128)(2,1)}) %all-gather.7.cloned.1.call-update) | async-done | bytes 2097168 | tf_op jit(solution)/shard_map/all_gather | solution.py:53
  160.3 8.7 %fusion.13 = f32[2048,256]{1,0:T(8,128)S(1)} fusion(bf16[2048,4096]{1,0:T(8,128)(2,1)} %param.17, bf16[4096,256]{1,0:T(8,128)(2,1)} %all-gather.7.cloned.1.call-done), kind=kOutput, calls=%fused_computation.34 | convolution fusion | flops 4294967296 | bytes 20971520 | tf_op jit(solution)/shard_map/dot_general | solution.py:51
  169.0 0.5 fusion.4
  169.5 1.2 convolution_add_fusion.1
  170.7 0.0 reduce-scatter.6.cloned.1.call-update
  170.7 0.0 copy-start.2
  170.7 0.0 reduce-scatter.4.cloned.1.call-start
  170.8 39.5 %all-gather.5.cloned.1.call-done = bf16[4096,256]{1,0:T(8,128)(2,1)} async-done(((bf16[512,256]{1,0:T(8,128)(2,1)}), bf16[4096,256]{1,0:T(8,128)(2,1)}) %all-gather.5.cloned.1.call-update) | async-done | bytes 2097168 | tf_op jit(solution)/shard_map/all_gather | solution.py:48
  210.3 8.7 %fusion.12 = f32[2048,256]{1,0:T(8,128)S(1)} fusion(bf16[2048,4096]{1,0:T(8,128)(2,1)} %param.17, bf16[4096,256]{1,0:T(8,128)(2,1)} %all-gather.5.cloned.1.call-done), kind=kOutput, calls=%fused_computation.33 | convolution fusion | flops 4294967296 | bytes 20971520 | tf_op jit(solution)/shard_map/dot_general | solution.py:46
  219.0 0.5 fusion.7
  219.5 0.0 copy-start.6
  219.5 0.0 copy-start.10
  219.5 0.0 copy-start.11
  219.5 0.0 copy-start.12
  219.5 0.0 copy-start.13
  219.6 0.0 copy-start.3
  219.6 1.2 convolution_add_fusion.2
  220.8 0.0 reduce-scatter.4.cloned.1.call-update
  220.8 0.0 all-gather.9.cloned.1.call-start
  220.9 1.0 multiply_reduce_fusion.2
  221.8 52.9 %reduce-scatter.6.cloned.1.call-done = f32[32,256]{1,0:T(8,128)} async-done(((f32[256,256]{1,0:T(8,128)}), f32[32,256]{1,0:T(8,128)}) %reduce-scatter.6.cloned.1.call-update) | async-done | bytes 32784 | tf_op jit(solution)/shard_map/reduce_scatter | solution.py:67
  274.7 1.4 add_divide_fusion.1
  276.1 30.9 %all_gather.30 = f32[256,256]{1,0:T(8,128)S(1)} all-gather(f32[32,256]{1,0:T(8,128)S(1)} %get-tuple-element.36), channel_id=1, replica_groups=mesh['fs'=8,'tp'=4] {'fs'}, dimensions={0}, use_global_device_ids=true | all-gather | bytes 294912 | tf_op jit(solution)/shard_map/all_gather | solution.py:75
  307.1 32.6 %reduce-scatter.4.cloned.1.call-done = f32[32,256]{1,0:T(8,128)} async-done(((f32[256,256]{1,0:T(8,128)}), f32[32,256]{1,0:T(8,128)}) %reduce-scatter.4.cloned.1.call-update) | async-done | bytes 32784 | tf_op jit(solution)/shard_map/reduce_scatter | solution.py:66
  339.6 1.4 add_divide_fusion.2
  341.0 30.8 %all_gather.28 = f32[256,256]{1,0:T(8,128)S(1)} all-gather(f32[32,256]{1,0:T(8,128)S(1)} %get-tuple-element.39), channel_id=1, replica_groups=mesh['fs'=8,'tp'=4] {'fs'}, dimensions={0}, use_global_device_ids=true | all-gather | bytes 294912 | tf_op jit(solution)/shard_map/all_gather | solution.py:74
  371.9 1.2 multiply_reduce_fusion.1
  373.1 1.2 multiply_reduce_fusion
  374.3 38.0 %all-reduce = (f32[]{:T(128)}, f32[]{:T(128)}, f32[]{:T(128)}) all-reduce(f32[]{:T(128)} %get-tuple-element.42, f32[]{:T(128)} %get-tuple-element.44, f32[]{:T(128)} %get-tuple-element.46), channel_id=1, replica_groups=mesh['fs'=8,'tp'=4] {'fs','tp'}, use_global_device_ids=true, to_apply=%region_2.0 | all-reduce | flops 3 | bytes 24 | tf_op jit(solution)/shard_map/psum | solution.py:81
  412.9 0.8 fusion.11
  413.7 0.0 all-gather.9.cloned.1.call-update
  413.8 0.0 all-gather.11.cloned.1.call-start
  413.8 1.2 copy.30
  415.7 0.8 fusion.10
  416.6 0.0 all-gather.11.cloned.1.call-update
  416.6 0.1 copy.31
  417.4 0.8 copy.34
  418.2 29.7 %all_gather.35 = bf16[1024,256]{0,1:T(8,128)(2,1)S(1)} all-gather(bf16[128,256]{0,1:T(8,128)(2,1)S(1)} %get-tuple-element.27), channel_id=1, replica_groups=mesh['fs'=8,'tp'=4] {'fs'}, dimensions={0}, use_global_device_ids=true | all-gather | bytes 589824 | tf_op jit(solution)/shard_map/all_gather | solution.py:93
  447.9 1.0 copy.37
  448.9 1.0 copy.32
  449.9 1.0 copy.33
  450.9 19.2 %all-gather.9.cloned.1.call-done = bf16[4096,256]{0,1:T(8,128)(2,1)} async-done(((bf16[512,256]{0,1:T(8,128)(2,1)}), bf16[4096,256]{0,1:T(8,128)(2,1)}) %all-gather.9.cloned.1.call-update) | async-done | bytes 2097168 | tf_op jit(solution)/shard_map/all_gather | solution.py:91
  470.1 4.1 copy.35
  474.2 46.5 %all-gather.11.cloned.1.call-done = bf16[4096,256]{0,1:T(8,128)(2,1)} async-done(((bf16[512,256]{0,1:T(8,128)(2,1)}), bf16[4096,256]{0,1:T(8,128)(2,1)}) %all-gather.11.cloned.1.call-update) | async-done | bytes 2097168 | tf_op jit(solution)/shard_map/all_gather | solution.py:92
  520.7 4.1 copy.36
  (18 shorter events, 0.1 us)
Async XLA Ops:
  7.2 36.9 %copy-start = (bf16[2048,256]{1,0:T(8,128)(2,1)S(1)}, bf16[2048,256]{1,0:T(8,128)(2,1)}, u32[]{:S(2)}) copy-start(bf16[2048,256]{1,0:T(8,128)(2,1)} %param.21) | copy-start | bytes 3145732
  7.2 102.0 %reduce-scatter.8.cloned.1.call-start = ((), (), s32[]{:S(2)}) async-start(), calls=%async_computation.7 | async-start | bytes 294912 | tf_op jit(solution)/shard_map/reduce_scatter | solution.py:68
  44.6 2.8 copy-start.5
  44.6 64.6 %copy-start.8 = (f32[32,256]{1,0:T(8,128)S(1)}, f32[32,256]{1,0:T(8,128)}, u32[]{:S(2)}) copy-start(f32[32,256]{1,0:T(8,128)} %param.33) | copy-start | bytes 98308
  44.6 64.6 %copy-start.9 = (f32[32,256]{1,0:T(8,128)S(1)}, f32[32,256]{1,0:T(8,128)}, u32[]{:S(2)}) copy-start(f32[32,256]{1,0:T(8,128)} %param.30) | copy-start | bytes 98308
  45.8 114.4 %all-gather.7.cloned.1.call-start = ((), (), s32[]{:S(2)}) async-start(), calls=%async_computation.5 | async-start | bytes 2359296 | tf_op jit(solution)/shard_map/all_gather | solution.py:53
  46.6 163.7 %all-gather.5.cloned.1.call-start = ((), (), s32[]{:S(2)}) async-start(), calls=%async_computation.3 | async-start | bytes 2359296 | tf_op jit(solution)/shard_map/all_gather | solution.py:48
  47.3 227.4 %reduce-scatter.6.cloned.1.call-start = ((), (), s32[]{:S(2)}) async-start(), calls=%async_computation.6 | async-start | bytes 294912 | tf_op jit(solution)/shard_map/reduce_scatter | solution.py:67
  142.0 27.0 %copy-start.1 = (bf16[2048,256]{1,0:T(8,128)(2,1)S(1)}, bf16[2048,256]{1,0:T(8,128)(2,1)}, u32[]{:S(2)}) copy-start(bf16[2048,256]{1,0:T(8,128)(2,1)} %param.19) | copy-start | bytes 3145732
  170.7 48.2 %copy-start.2 = (bf16[2048,256]{1,0:T(8,128)(2,1)S(1)}, bf16[2048,256]{1,0:T(8,128)(2,1)}, u32[]{:S(2)}) copy-start(bf16[2048,256]{1,0:T(8,128)(2,1)} %param.18) | copy-start | bytes 3145732
  170.7 168.9 %reduce-scatter.4.cloned.1.call-start = ((), (), s32[]{:S(2)}) async-start(), calls=%async_computation.4 | async-start | bytes 294912 | tf_op jit(solution)/shard_map/reduce_scatter | solution.py:66
  219.5 1.4 copy-start.6
  219.5 55.2 %copy-start.10 = (f32[32,256]{1,0:T(8,128)S(1)}, f32[32,256]{1,0:T(8,128)}, u32[]{:S(2)}) copy-start(f32[32,256]{1,0:T(8,128)} %param.32) | copy-start | bytes 98308
  219.5 55.2 %copy-start.11 = (f32[32,256]{1,0:T(8,128)S(1)}, f32[32,256]{1,0:T(8,128)}, u32[]{:S(2)}) copy-start(f32[32,256]{1,0:T(8,128)} %param.29) | copy-start | bytes 98308
  219.5 120.1 %copy-start.12 = (f32[32,256]{1,0:T(8,128)S(1)}, f32[32,256]{1,0:T(8,128)}, u32[]{:S(2)}) copy-start(f32[32,256]{1,0:T(8,128)} %param.31) | copy-start | bytes 98308
  219.5 120.1 %copy-start.13 = (f32[32,256]{1,0:T(8,128)S(1)}, f32[32,256]{1,0:T(8,128)}, u32[]{:S(2)}) copy-start(f32[32,256]{1,0:T(8,128)} %param.28) | copy-start | bytes 98308
  219.6 152.3 %copy-start.3 = (bf16[512,256]{1,0:T(8,128)(2,1)S(1)}, bf16[512,256]{1,0:T(8,128)(2,1)}, u32[]{:S(2)}) copy-start(bf16[512,256]{1,0:T(8,128)(2,1)} %param.25) | copy-start | bytes 786436
  220.8 152.3 %copy-start.4 = (bf16[512,256]{1,0:T(8,128)(2,1)S(1)}, bf16[512,256]{1,0:T(8,128)(2,1)}, u32[]{:S(2)}) copy-start(bf16[512,256]{1,0:T(8,128)(2,1)} %param.26) | copy-start | bytes 786436
  220.8 249.3 %all-gather.9.cloned.1.call-start = ((), (), s32[]{:S(2)}) async-start(), calls=%async_computation.8 | async-start | bytes 2359296 | tf_op jit(solution)/shard_map/all_gather | solution.py:91
  413.7 2.9 copy-start.7
  413.8 106.9 %all-gather.11.cloned.1.call-start = ((), (), s32[]{:S(2)}) async-start(), calls=%async_computation.9 | async-start | bytes 2359296 | tf_op jit(solution)/shard_map/all_gather | solution.py:92
Sparse Core Ops, SparseCore 0:
  46.0 63.1 reduce-scatter.7
  111.3 48.9 all-gather.6
  162.4 47.8 all-gather.4
  214.0 60.6 reduce-scatter.5
  278.5 61.1 reduce-scatter.3
  413.9 56.1 all-gather.8
  472.1 48.5 all-gather.10
where the time goes:
time: 532 us
  waiting for transfers between devices  272 us (51%)
  blocking collectives  194 us (36%)
  matrix products  29.3 us (6%)
  between operations  16.4 us (3%)
  local copies, waits for them, and re-layouts  13.5 us (3%)
  other arithmetic  5.86 us (1%)
    reduce_scatter x1, waiting for transfers between devices, local(): lax.psum_scatter(low_point, 'fs', scatter_dimension=0, tiled=True)  61.6 us
    reduce_scatter x1, waiting for transfers between devices, local(): lax.psum_scatter(low_gate, 'fs', scatter_dimension=0, tiled=True)  52.9 us
    all_gather x1, waiting for transfers between devices, local(): lax.all_gather(new_g.astype(jnp.bfloat16), 'fs', axis=0, tiled=True)  46.5 us
    all_gather x1, waiting for transfers between devices, local(): lax.all_gather(factor_value, 'fs', axis=0, tiled=True)  39.5 us
    psum x1, blocking collectives, local(): lax.psum((jnp.sum(full_v * full_v), jnp.sum(full_g * full_g), jnp.sum(ful...  38 us
    all_gather x1, blocking collectives, local(): lax.all_gather(factor_point, 'fs', axis=0, tiled=True)  33.4 us
    reduce_scatter x1, waiting for transfers between devices, local(): lax.psum_scatter(low_value, 'fs', scatter_dimension=0, tiled=True)  32.6 us
    all_gather x1, blocking collectives, local(): lax.all_gather(dpt, 'fs', axis=0, tiled=True)  31.4 us
  transfers between devices with their start and end apart: 7, of which 7 were waited for; matrix products, arithmetic and copies ran while one was open for 7% of the time, Pallas kernels for 0%

commit v1 on v0

--- a/solution.py
+++ b/solution.py
@@ -2,6 +2,24 @@
 import jax.numpy as jnp
 from jax import lax
 from jax.sharding import PartitionSpec as P
+
+
+def ring_gather(array, axis, dim):
+    ways, here, step = (lax.axis_size(axis), lax.axis_index(axis), array.shape[dim])
+    shape = [n * ways if d == dim else n for d, n in enumerate(array.shape)]
+    full = lax.dynamic_update_slice_in_dim(
+        jnp.zeros(shape, array.dtype), array, here * step, axis=dim
+    )
+    going_up = going_down = array
+    for far in range(1, ways // 2 + 1):
+        going_up = lax.ppermute(going_up, axis, [(d, (d + 1) % ways) for d in range(ways)])
+        full = lax.dynamic_update_slice_in_dim(full, going_up, (here - far) % ways * step, axis=dim)
+        if 2 * far < ways:
+            going_down = lax.ppermute(going_down, axis, [(d, (d - 1) % ways) for d in range(ways)])
+            full = lax.dynamic_update_slice_in_dim(
+                full, going_down, (here + far) % ways * step, axis=dim
+            )
+    return full
 
 
 def contract_rows(left, right):
@@ -72,7 +90,7 @@
     fpt, spt, dpt = moments(summed[2] / total, first_point, second_point)
     whole_v, whole_g, whole_p = (
         lax.all_gather(dv, "fs", axis=0, tiled=True),
-        lax.all_gather(dg, "fs", axis=0, tiled=True),
+        ring_gather(dg, "fs", 0),
         lax.all_gather(dpt, "fs", axis=0, tiled=True),
     )
     full_v = jnp.dot(factor_value.astype(jnp.float32), whole_v, precision=lax.Precision.HIGHEST)

time: 532 us -> 551 us (1.036)
  waiting for transfers between devices: 272 us -> 308 us
  blocking collectives: 194 us -> 163 us
  starting transfers between devices: 0.28 us -> 14.5 us
    all_gather x1 -> x0, blocking collectives: 30.9 us -> none  [local(): lax.all_gather(dg, 'fs', axis=0, tiled=True)]
    reduce_scatter x1, waiting for transfers between devices: 52.9 us -> 22 us  [local(): lax.psum_scatter(low_gate, 'fs', scatter_dimension=0, tiled=True)]
    all_gather x1, waiting for transfers between devices: 18.3 us -> 48.9 us  [local(): lax.all_gather(factor_gate, 'fs', axis=0, tiled=True)]
    reduce_scatter x1, waiting for transfers between devices: 32.6 us -> 58.8 us  [local(): lax.psum_scatter(low_value, 'fs', scatter_dimension=0, tiled=True)]
    ppermute x0 -> x7, starting transfers between devices: none -> 14.2 us  [the longest x3 12.7 us: ring_gather(): lax.ppermute(going_down, axis, [(d, (d - 1) % ways) for d in range(ways)])]
    ppermute x0 -> x7, waiting for transfers between devices: none -> 10.3 us  [the longest x4 10.3 us: ring_gather(): lax.ppermute(going_up, axis, [(d, (d + 1) % ways) for d in range(ways)])]
  transfers between devices with their start and end apart: 7 -> 14, of which waited for: 7 -> 10; matrix products, arithmetic and copies ran while one was open for 7% -> 7% of each run, Pallas kernels for 0% -> 0%
where the time goes in v1:
time: 551 us
  waiting for transfers between devices  308 us (56%)
  blocking collectives  163 us (30%)
  matrix products  29.3 us (5%)
  between operations  16.7 us (3%)
  starting transfers between devices  14.5 us (3%)
  local copies, waits for them, and re-layouts  13.5 us (2%)
  other arithmetic  5.85 us (1%)
    reduce_scatter x1, waiting for transfers between devices, local(): lax.psum_scatter(low_point, 'fs', scatter_dimension=0, tiled=True)  61.4 us
    reduce_scatter x1, waiting for transfers between devices, local(): lax.psum_scatter(low_value, 'fs', scatter_dimension=0, tiled=True)  58.8 us
    all_gather x1, waiting for transfers between devices, local(): lax.all_gather(factor_gate, 'fs', axis=0, tiled=True)  48.9 us
    all_gather x1, waiting for transfers between devices, local(): lax.all_gather(new_g.astype(jnp.bfloat16), 'fs', axis=0, tiled=True)  46.5 us
    all_gather x1, waiting for transfers between devices, local(): lax.all_gather(factor_value, 'fs', axis=0, tiled=True)  39.3 us
    psum x1, blocking collectives, local(): lax.psum((jnp.sum(full_v * full_v), jnp.sum(full_g * full_g), jnp.sum(ful...  37.3 us
    all_gather x1, blocking collectives, local(): lax.all_gather(factor_point, 'fs', axis=0, tiled=True)  33.4 us
    all_gather x1, blocking collectives, local(): lax.all_gather(dv, 'fs', axis=0, tiled=True)  31 us
  transfers between devices with their start and end apart: 14, of which 10 were waited for; matrix products, arithmetic and copies ran while one was open for 7% of the time, Pallas kernels for 0%

profile of v1, /device:TPU:0, one launch (start us, length us, event | category | flops | bytes accessed | tf_op | source)
XLA Modules:
  0.0 550.7 jit_solution(12630729554457841299)
XLA Ops:
  7.2 0.0 copy-start
  7.2 0.0 reduce-scatter.8.cloned.1.call-start
  7.2 33.4 %all_gather.27 = bf16[1024,256]{1,0:T(8,128)(2,1)S(1)} all-gather(bf16[128,256]{1,0:T(8,128)(2,1)} %param.27), channel_id=1, replica_groups=mesh['fs'=8,'tp'=4] {'fs'}, dimensions={0}, use_global_device_ids=true | all-gather | bytes 589824 | tf_op jit(solution)/shard_map/all_gather | solution.py:77
  40.6 3.5 fusion.14
  44.1 0.5 fusion.1
  44.6 0.0 copy-start.10
  44.6 0.0 copy-start.11
  44.6 1.2 convolution_add_fusion
  45.8 0.0 reduce-scatter.8.cloned.1.call-update
  45.9 0.0 all-gather.7.cloned.1.call-start
  45.9 0.7 all-gather.7.cloned.1.call-update
  46.6 0.0 all-gather.5.cloned.1.call-start
  46.7 0.7 all-gather.5.cloned.1.call-update
  47.3 0.0 reduce-scatter.6.cloned.1.call-start
  47.5 0.2 copy.29
  47.8 61.4 %reduce-scatter.8.cloned.1.call-done = f32[32,256]{1,0:T(8,128)} async-done(((f32[256,256]{1,0:T(8,128)}), f32[32,256]{1,0:T(8,128)}) %reduce-scatter.8.cloned.1.call-update) | async-done | bytes 32784 | tf_op jit(solution)/shard_map/reduce_scatter | solution.py:86
  109.2 1.4 add_divide_fusion
  110.6 48.9 %all-gather.7.cloned.1.call-done = bf16[4096,256]{1,0:T(8,128)(2,1)} async-done(((bf16[512,256]{1,0:T(8,128)(2,1)}), bf16[4096,256]{1,0:T(8,128)(2,1)}) %all-gather.7.cloned.1.call-update) | async-done | bytes 2097168 | tf_op jit(solution)/shard_map/all_gather | solution.py:71
  159.5 8.7 %fusion.13 = f32[2048,256]{1,0:T(8,128)S(1)} fusion(bf16[2048,4096]{1,0:T(8,128)(2,1)} %param.17, bf16[4096,256]{1,0:T(8,128)(2,1)} %all-gather.7.cloned.1.call-done), kind=kOutput, calls=%fused_computation.42 | convolution fusion | flops 4294967296 | bytes 20971520 | tf_op jit(solution)/shard_map/dot_general | solution.py:69
  168.2 0.5 fusion.4
  168.7 1.2 convolution_add_fusion.1
  169.9 0.0 reduce-scatter.6.cloned.1.call-update
  169.9 0.0 copy-start.2
  169.9 0.0 reduce-scatter.4.cloned.1.call-start
  170.0 39.3 %all-gather.5.cloned.1.call-done = bf16[4096,256]{1,0:T(8,128)(2,1)} async-done(((bf16[512,256]{1,0:T(8,128)(2,1)}), bf16[4096,256]{1,0:T(8,128)(2,1)}) %all-gather.5.cloned.1.call-update) | async-done | bytes 2097168 | tf_op jit(solution)/shard_map/all_gather | solution.py:66
  209.3 8.7 %fusion.12 = f32[2048,256]{1,0:T(8,128)S(1)} fusion(bf16[2048,4096]{1,0:T(8,128)(2,1)} %param.17, bf16[4096,256]{1,0:T(8,128)(2,1)} %all-gather.5.cloned.1.call-done), kind=kOutput, calls=%fused_computation.41 | convolution fusion | flops 4294967296 | bytes 20971520 | tf_op jit(solution)/shard_map/dot_general | solution.py:64
  218.0 0.5 fusion.7
  218.5 0.0 copy-start.9
  218.6 1.2 convolution_add_fusion.2
  219.8 0.0 reduce-scatter.4.cloned.1.call-update
  219.8 0.0 all-gather.9.cloned.1.call-start
  219.8 30.9 %all_gather.28 = f32[256,256]{1,0:T(8,128)S(1)} all-gather(f32[32,256]{1,0:T(8,128)S(1)} %get-tuple-element.33), channel_id=1, replica_groups=mesh['fs'=8,'tp'=4] {'fs'}, dimensions={0}, use_global_device_ids=true | all-gather | bytes 294912 | tf_op jit(solution)/shard_map/all_gather | solution.py:94
  250.7 1.0 multiply_reduce_fusion.2
  251.7 22.0 %reduce-scatter.6.cloned.1.call-done = f32[32,256]{1,0:T(8,128)} async-done(((f32[256,256]{1,0:T(8,128)}), f32[32,256]{1,0:T(8,128)}) %reduce-scatter.6.cloned.1.call-update) | async-done | bytes 32784 | tf_op jit(solution)/shard_map/reduce_scatter | solution.py:85
  273.7 1.4 constant_dynamic-update-slice_fusion.7
  275.1 1.4 collective-permute-start
  276.6 3.3 collective-permute-start.1
  279.9 58.8 %reduce-scatter.4.cloned.1.call-done = f32[32,256]{1,0:T(8,128)} async-done(((f32[256,256]{1,0:T(8,128)}), f32[32,256]{1,0:T(8,128)}) %reduce-scatter.4.cloned.1.call-update) | async-done | bytes 32784 | tf_op jit(solution)/shard_map/reduce_scatter | solution.py:84
  338.6 1.4 add_divide_fusion.2
  340.0 31.0 %all_gather.25 = f32[256,256]{1,0:T(8,128)S(1)} all-gather(f32[32,256]{1,0:T(8,128)S(1)} %get-tuple-element.40), channel_id=1, replica_groups=mesh['fs'=8,'tp'=4] {'fs'}, dimensions={0}, use_global_device_ids=true | all-gather | bytes 294912 | tf_op jit(solution)/shard_map/all_gather | solution.py:92
  371.0 1.2 multiply_reduce_fusion.1
  372.2 4.7 collective-permute-start.3
  377.0 1.9 collective-permute-done.2
  378.9 4.7 collective-permute-start.5
  383.6 1.9 collective-permute-done.4
  385.5 6.6 %collective-permute-done.6 = f32[32,256]{1,0:T(8,128)S(1)} collective-permute-done((f32[32,256]{1,0:T(8,128)S(1)}, f32[32,256]{1,0:T(8,128)S(1)}, u32[]{:S(2)}, u32[]{:S(2)}) %collective-permute-start.6) | collective-permute-done | bytes 32800 | tf_op jit(solution)/shard_map/ppermute | solution.py:15
  392.1 1.2 multiply_reduce_fusion
  393.3 37.3 %all-reduce = (f32[]{:T(128)}, f32[]{:T(128)}, f32[]{:T(128)}) all-reduce(f32[]{:T(128)} %get-tuple-element.43, f32[]{:T(128)} %get-tuple-element.45, f32[]{:T(128)} %get-tuple-element.47), channel_id=1, replica_groups=mesh['fs'=8,'tp'=4] {'fs','tp'}, use_global_device_ids=true, to_apply=%region_2.0 | all-reduce | flops 3 | bytes 24 | tf_op jit(solution)/shard_map/psum | solution.py:99
  431.3 0.8 fusion.11
  432.1 0.0 all-gather.9.cloned.1.call-update
  432.1 0.0 all-gather.11.cloned.1.call-start
  432.2 1.2 copy.30
  434.1 0.8 fusion.10
  434.9 0.0 all-gather.11.cloned.1.call-update
  435.0 0.1 copy.31
  435.8 0.8 copy.34
  436.6 30.0 %all_gather.31 = bf16[1024,256]{0,1:T(8,128)(2,1)S(1)} all-gather(bf16[128,256]{0,1:T(8,128)(2,1)S(1)} %get-tuple-element.27), channel_id=1, replica_groups=mesh['fs'=8,'tp'=4] {'fs'}, dimensions={0}, use_global_device_ids=true | all-gather | bytes 589824 | tf_op jit(solution)/shard_map/all_gather | solution.py:111
  466.5 1.0 copy.37
  467.5 1.0 copy.32
  468.5 1.0 copy.33
  469.5 19.7 %all-gather.9.cloned.1.call-done = bf16[4096,256]{0,1:T(8,128)(2,1)} async-done(((bf16[512,256]{0,1:T(8,128)(2,1)}), bf16[4096,256]{0,1:T(8,128)(2,1)}) %all-gather.9.cloned.1.call-update) | async-done | bytes 2097168 | tf_op jit(solution)/shard_map/all_gather | solution.py:109
  489.2 4.1 copy.35
  493.3 46.5 %all-gather.11.cloned.1.call-done = bf16[4096,256]{0,1:T(8,128)(2,1)} async-done(((bf16[512,256]{0,1:T(8,128)(2,1)}), bf16[4096,256]{0,1:T(8,128)(2,1)}) %all-gather.11.cloned.1.call-update) | async-done | bytes 2097168 | tf_op jit(solution)/shard_map/all_gather | solution.py:110
  539.8 4.1 copy.36
  (39 shorter events, 0.2 us)
Async XLA Ops:
  7.2 36.9 %copy-start = (bf16[2048,256]{1,0:T(8,128)(2,1)S(1)}, bf16[2048,256]{1,0:T(8,128)(2,1)}, u32[]{:S(2)}) copy-start(bf16[2048,256]{1,0:T(8,128)(2,1)} %param.21) | copy-start | bytes 3145732
  7.2 102.0 %reduce-scatter.8.cloned.1.call-start = ((), (), s32[]{:S(2)}) async-start(), calls=%async_computation.7 | async-start | bytes 294912 | tf_op jit(solution)/shard_map/reduce_scatter | solution.py:86
  44.6 2.9 copy-start.5
  44.6 64.6 %copy-start.10 = (f32[32,256]{1,0:T(8,128)S(1)}, f32[32,256]{1,0:T(8,128)}, u32[]{:S(2)}) copy-start(f32[32,256]{1,0:T(8,128)} %param.33) | copy-start | bytes 98308
  44.6 64.6 %copy-start.11 = (f32[32,256]{1,0:T(8,128)S(1)}, f32[32,256]{1,0:T(8,128)}, u32[]{:S(2)}) copy-start(f32[32,256]{1,0:T(8,128)} %param.30) | copy-start | bytes 98308
  45.9 113.6 %all-gather.7.cloned.1.call-start = ((), (), s32[]{:S(2)}) async-start(), calls=%async_computation.5 | async-start | bytes 2359296 | tf_op jit(solution)/shard_map/all_gather | solution.py:71
  46.6 162.6 %all-gather.5.cloned.1.call-start = ((), (), s32[]{:S(2)}) async-start(), calls=%async_computation.3 | async-start | bytes 2359296 | tf_op jit(solution)/shard_map/all_gather | solution.py:66
  47.3 226.4 %reduce-scatter.6.cloned.1.call-start = ((), (), s32[]{:S(2)}) async-start(), calls=%async_computation.6 | async-start | bytes 294912 | tf_op jit(solution)/shard_map/reduce_scatter | solution.py:85
  110.6 57.6 %copy-start.1 = (bf16[2048,256]{1,0:T(8,128)(2,1)S(1)}, bf16[2048,256]{1,0:T(8,128)(2,1)}, u32[]{:S(2)}) copy-start(bf16[2048,256]{1,0:T(8,128)(2,1)} %param.19) | copy-start | bytes 3145732
  169.9 48.1 %copy-start.2 = (bf16[2048,256]{1,0:T(8,128)(2,1)S(1)}, bf16[2048,256]{1,0:T(8,128)(2,1)}, u32[]{:S(2)}) copy-start(bf16[2048,256]{1,0:T(8,128)(2,1)} %param.18) | copy-start | bytes 3145732
  169.9 168.7 %reduce-scatter.4.cloned.1.call-start = ((), (), s32[]{:S(2)}) async-start(), calls=%async_computation.4 | async-start | bytes 294912 | tf_op jit(solution)/shard_map/reduce_scatter | solution.py:84
  218.5 32.2 %copy-start.6 = (bf16[128,256]{1,0:T(8,128)(2,1)S(1)}, bf16[128,256]{1,0:T(8,128)(2,1)}, u32[]{:S(2)}) copy-start(bf16[128,256]{1,0:T(8,128)(2,1)} %param.27) | copy-start | bytes 196612
  218.5 55.2 %copy-start.8 = (f32[32,256]{1,0:T(8,128)S(1)}, f32[32,256]{1,0:T(8,128)}, u32[]{:S(2)}) copy-start(f32[32,256]{1,0:T(8,128)} %param.32) | copy-start | bytes 98308
  218.5 55.2 %copy-start.9 = (f32[32,256]{1,0:T(8,128)S(1)}, f32[32,256]{1,0:T(8,128)}, u32[]{:S(2)}) copy-start(f32[32,256]{1,0:T(8,128)} %param.29) | copy-start | bytes 98308
  218.5 120.1 %copy-start.12 = (f32[32,256]{1,0:T(8,128)S(1)}, f32[32,256]{1,0:T(8,128)}, u32[]{:S(2)}) copy-start(f32[32,256]{1,0:T(8,128)} %param.31) | copy-start | bytes 98308
  218.5 120.1 %copy-start.13 = (f32[32,256]{1,0:T(8,128)S(1)}, f32[32,256]{1,0:T(8,128)}, u32[]{:S(2)}) copy-start(f32[32,256]{1,0:T(8,128)} %param.28) | copy-start | bytes 98308
  218.5 152.5 %copy-start.3 = (bf16[512,256]{1,0:T(8,128)(2,1)S(1)}, bf16[512,256]{1,0:T(8,128)(2,1)}, u32[]{:S(2)}) copy-start(bf16[512,256]{1,0:T(8,128)(2,1)} %param.25) | copy-start | bytes 786436
  219.8 172.3 %copy-start.4 = (bf16[512,256]{1,0:T(8,128)(2,1)S(1)}, bf16[512,256]{1,0:T(8,128)(2,1)}, u32[]{:S(2)}) copy-start(bf16[512,256]{1,0:T(8,128)(2,1)} %param.26) | copy-start | bytes 786436
  219.8 269.4 %all-gather.9.cloned.1.call-start = ((), (), s32[]{:S(2)}) async-start(), calls=%async_computation.8 | async-start | bytes 2359296 | tf_op jit(solution)/shard_map/all_gather | solution.py:109
  275.1 97.1 %collective-permute-start = (f32[32,256]{1,0:T(8,128)S(1)}, f32[32,256]{1,0:T(8,128)S(1)}, u32[]{:S(2)}, u32[]{:S(2)}) collective-permute-start(f32[32,256]{1,0:T(8,128)S(1)} %get-tuple-element.37), channel_id=1, source_target_pairs={{0,4},{4,8},{8,12},{12,16},{16,20},{20,24},{24,28},{28,0},{1,5},{5... | collective-permute-start | bytes 98312 | tf_op jit(solution)/shard_map/ppermute | solution.py:15
  276.6 95.7 %collective-permute-start.1 = (f32[32,256]{1,0:T(8,128)S(1)}, f32[32,256]{1,0:T(8,128)S(1)}, u32[]{:S(2)}, u32[]{:S(2)}) collective-permute-start(f32[32,256]{1,0:T(8,128)S(1)} %get-tuple-element.37), channel_id=1, source_target_pairs={{0,28},{4,0},{8,4},{12,8},{16,12},{20,16},{24,20},{28,24},{1,29},{... | collective-permute-start | bytes 98312 | tf_op jit(solution)/shard_map/ppermute | solution.py:18
  372.2 6.6 %collective-permute-start.2 = (f32[32,256]{1,0:T(8,128)S(1)}, f32[32,256]{1,0:T(8,128)S(1)}, u32[]{:S(2)}, u32[]{:S(2)}) collective-permute-start(f32[32,256]{1,0:T(8,128)S(1)} %collective-permute-done), channel_id=1, source_target_pairs={{0,4},{4,8},{8,12},{12,16},{16,20},{20,24},{24,28},{28,0},{1,5},{5... | collective-permute-start | bytes 98312 | tf_op jit(solution)/shard_map/ppermute | solution.py:15
  372.2 6.6 %collective-permute-start.3 = (f32[32,256]{1,0:T(8,128)S(1)}, f32[32,256]{1,0:T(8,128)S(1)}, u32[]{:S(2)}, u32[]{:S(2)}) collective-permute-start(f32[32,256]{1,0:T(8,128)S(1)} %collective-permute-done.1), channel_id=1, source_target_pairs={{0,28},{4,0},{8,4},{12,8},{16,12},{20,16},{24,20},{28,24},{1,29},{... | collective-permute-start | bytes 98312 | tf_op jit(solution)/shard_map/ppermute | solution.py:18
  378.9 6.6 %collective-permute-start.4 = (f32[32,256]{1,0:T(8,128)S(1)}, f32[32,256]{1,0:T(8,128)S(1)}, u32[]{:S(2)}, u32[]{:S(2)}) collective-permute-start(f32[32,256]{1,0:T(8,128)S(1)} %collective-permute-done.2), channel_id=1, source_target_pairs={{0,4},{4,8},{8,12},{12,16},{16,20},{20,24},{24,28},{28,0},{1,5},{5... | collective-permute-start | bytes 98312 | tf_op jit(solution)/shard_map/ppermute | solution.py:15
  378.9 6.6 %collective-permute-start.5 = (f32[32,256]{1,0:T(8,128)S(1)}, f32[32,256]{1,0:T(8,128)S(1)}, u32[]{:S(2)}, u32[]{:S(2)}) collective-permute-start(f32[32,256]{1,0:T(8,128)S(1)} %collective-permute-done.3), channel_id=1, source_target_pairs={{0,28},{4,0},{8,4},{12,8},{16,12},{20,16},{24,20},{28,24},{1,29},{... | collective-permute-start | bytes 98312 | tf_op jit(solution)/shard_map/ppermute | solution.py:18
  385.5 6.6 %collective-permute-start.6 = (f32[32,256]{1,0:T(8,128)S(1)}, f32[32,256]{1,0:T(8,128)S(1)}, u32[]{:S(2)}, u32[]{:S(2)}) collective-permute-start(f32[32,256]{1,0:T(8,128)S(1)} %collective-permute-done.4), channel_id=1, source_target_pairs={{0,4},{4,8},{8,12},{12,16},{16,20},{20,24},{24,28},{28,0},{1,5},{5... | collective-permute-start | bytes 98312 | tf_op jit(solution)/shard_map/ppermute | solution.py:15
  432.1 2.9 copy-start.7
  432.1 107.7 %all-gather.11.cloned.1.call-start = ((), (), s32[]{:S(2)}) async-start(), calls=%async_computation.9 | async-start | bytes 2359296 | tf_op jit(solution)/shard_map/all_gather | solution.py:110
Sparse Core Ops, SparseCore 0:
  46.0 63.1 reduce-scatter.7
  111.3 48.1 all-gather.6
  161.6 47.6 all-gather.4
  213.0 60.6 reduce-scatter.5
  277.4 61.1 reduce-scatter.3
  432.3 56.9 all-gather.8
  491.3 48.5 all-gather.10
